TPU v7x, 32 devices: a whole 2x2x4 slice. The times are simulated.
32 devices in a mesh: ep: 8 (over z, x), tp: 4 (over y, core).
Axes of the slice: x: 2, y: 2, z: 4, core: 2. Of those that a mesh axis runs over, the one named last changes fastest.
Arguments:
- conv_value: bfloat16 [4096, 2048], P('ep', 'tp'), may hold values from -6 to 6
- conv_gate: bfloat16 [4096, 2048], P('ep', 'tp'), may hold values from -9 to 9
- conv_taps: float32 [31, 2048], P(None, 'tp'), may hold values from -14 to 14
- norm_gain: float32 [2048], P('tp'), may hold values from 0.1 to 1.9
- norm_shift: float32 [2048], P('tp'), may hold values from -3 to 3
- conv_out_weight: bfloat16 [2048, 2048], P(None, 'tp'), may hold values from -0.125 to 0.125
- moe_input: bfloat16 [1024, 2048], P('ep'), may hold values from -6 to 6
- moe_gain: float32 [2048], replicated, may hold values from 0.1 to 1.9
- routes: int32 [1024, 4], P('ep'), may hold values from 0 to 7, all different within a row; in each aligned block of 128 rows (0 to 127, 128 to 255, ...) at most 128 rows name the same one
- route_weights: float32 [1024, 4], P('ep'), may hold values from 0.25 to 1
- expert_gate: bfloat16 [8, 2048, 4096], P('ep', None, 'tp'), may hold values from -0.125 to 0.125
- expert_up: bfloat16 [8, 2048, 4096], P('ep', None, 'tp'), may hold values from -0.125 to 0.125
- expert_down: bfloat16 [8, 4096, 2048], P('ep', None, 'tp'), may hold values from -0.09375 to 0.09375
- shared_gate: bfloat16 [2048, 512], P(None, 'tp'), may hold values from -0.125 to 0.125
- shared_up: bfloat16 [2048, 512], P(None, 'tp'), may hold values from -0.125 to 0.125
- shared_down: bfloat16 [512, 2048], P(None, 'tp'), may hold values from -0.25 to 0.25
Outputs:
- conv_result: bfloat16 [4096, 2048], P('ep', 'tp')
- moe_result: bfloat16 [1024, 2048], P('ep', 'tp')
Inputs may be any that keep to these rules, and one draw needn't show every extreme that they name: `routes`: in the rows of one device (aligned blocks of 128 rows) no expert is named by more than 128 rows, a bound that some block reaches; each row names 4 different experts.
All inputs are finite; a program needn't handle non-finite values.
Results may differ from a plain program's by a relative error of at most 0.0068.
Values may be sent and summed in bfloat16 or wider, within the bound.
A program may use at most 64 MiB of HBM per device.

v0:
```python
import jax
import jax.numpy as jnp
from jax import lax
from jax.sharding import PartitionSpec as P


def from_behind(value, axis, steps):
    count = lax.axis_size(axis)
    initial, last = (max(0, -steps), min(count, count - steps))
    return lax.ppermute(value, axis, [(source, source + steps) for source in range(initial, last)])


def body(
    conv_value,
    conv_gate,
    conv_taps,
    norm_gain,
    norm_shift,
    conv_out_weight,
    moe_input,
    moe_gain,
    routes,
    route_weights,
    expert_gate,
    expert_up,
    expert_down,
    shared_gate,
    shared_up,
    shared_down,
):
    tap_count = conv_taps.shape[0]
    rows_a = conv_value.shape[0]
    glu_rows = (
        conv_value.astype(jnp.float32) * jax.nn.sigmoid(conv_gate.astype(jnp.float32))
    ).astype(jnp.bfloat16)
    before = from_behind(glu_rows[rows_a - (tap_count - 1) :], "ep", 1)
    padded = jnp.concatenate([before, glu_rows], axis=0)
    filtered = jnp.zeros(glu_rows.shape, jnp.float32)
    for offset in range(tap_count):
        filtered = filtered + conv_taps[offset] * padded[offset : offset + rows_a].astype(
            jnp.float32
        )
    row_total, squares = lax.psum(
        (jnp.sum(filtered, axis=1), jnp.sum(filtered * filtered, axis=1)), "tp"
    )
    channels = conv_out_weight.shape[0]
    row_mean = row_total / channels
    row_square = squares / channels
    scaled = (filtered - row_mean[:, None]) * lax.rsqrt(row_square - row_mean * row_mean + 1e-05)[
        :, None
    ]
    conv_hidden = jax.nn.silu(scaled * norm_gain + norm_shift).astype(jnp.bfloat16)
    conv_sum = jnp.dot(
        lax.all_gather(conv_hidden, "tp", axis=1, tiled=True),
        conv_out_weight,
        preferred_element_type=jnp.float32,
    )
    conv_result = conv_sum.astype(jnp.bfloat16)
    inputs = moe_input.astype(jnp.float32)
    normed = (
        inputs * lax.rsqrt(jnp.mean(inputs * inputs, axis=1, keepdims=True) + 1e-06) * moe_gain
    ).astype(jnp.bfloat16)
    rows_b, per_row = routes.shape
    model_width = normed.shape[1]
    groups = lax.axis_size("ep")
    capacity = 2 * rows_b * per_row // groups
    flat_expert = routes.reshape(-1)
    owner_row = jnp.arange(rows_b * per_row, dtype=jnp.int32) // per_row
    expert_hits = (flat_expert[:, None] == jnp.arange(groups, dtype=jnp.int32)[None, :]).astype(
        jnp.int32
    )
    slot_rank = jnp.sum((jnp.cumsum(expert_hits, axis=0) - expert_hits) * expert_hits, axis=1)
    slot_index = flat_expert * capacity + slot_rank
    outgoing = (
        jnp.zeros((groups * capacity, model_width), jnp.bfloat16)
        .at[slot_index]
        .set(normed[owner_row])
    )
    outgoing = outgoing.reshape(groups, capacity, model_width)
    slot_share = capacity // lax.axis_size("tp")
    own_slots = lax.dynamic_slice_in_dim(outgoing, lax.axis_index("tp") * slot_share, slot_share, 1)
    partial_rows = lax.all_to_all(own_slots, "ep", split_axis=0, concat_axis=0, tiled=True)
    arrived = lax.all_gather(partial_rows, "tp", axis=1, tiled=True)
    arrived_rows = arrived.reshape(groups * capacity, model_width)
    gate_value = jnp.dot(arrived_rows, expert_gate[0], preferred_element_type=jnp.float32)
    upward = jnp.dot(arrived_rows, expert_up[0], preferred_element_type=jnp.float32)
    expert_hidden = (jax.nn.silu(gate_value) * upward).astype(jnp.bfloat16)
    shared_hidden = (
        jax.nn.silu(jnp.dot(normed, shared_gate, preferred_element_type=jnp.float32))
        * jnp.dot(normed, shared_up, preferred_element_type=jnp.float32)
    ).astype(jnp.bfloat16)
    columns = expert_down.shape[2]
    routed_rows = expert_down[0]
    routed_sum = jnp.dot(
        lax.all_gather(expert_hidden, "tp", axis=1, tiled=True),
        routed_rows,
        preferred_element_type=jnp.float32,
    )
    shared_sum = jnp.dot(
        lax.all_gather(shared_hidden, "tp", axis=1, tiled=True),
        shared_down,
        preferred_element_type=jnp.float32,
    )
    expert_out = routed_sum.astype(jnp.bfloat16).reshape(groups, capacity, columns)
    returned = lax.all_to_all(expert_out, "ep", split_axis=0, concat_axis=0, tiled=True).reshape(
        groups * capacity, columns
    )
    picked = returned[slot_index].astype(jnp.float32) * route_weights.reshape(-1)[:, None]
    moe_sum = jnp.sum(picked.reshape(rows_b, per_row, columns), axis=1) + shared_sum
    return (conv_result, moe_sum.astype(jnp.bfloat16))


def solution(mesh):
    return jax.shard_map(
        body,
        mesh=mesh,
        in_specs=(
            P("ep", "tp"),
            P("ep", "tp"),
            P(None, "tp"),
            P("tp"),
            P("tp"),
            P(None, "tp"),
            P("ep", None),
            P(),
            P("ep", None),
            P("ep", None),
            P("ep", None, "tp"),
            P("ep", None, "tp"),
            P("ep", None, "tp"),
            P(None, "tp"),
            P(None, "tp"),
            P(None, "tp"),
        ),
        out_specs=(P("ep", "tp"), P("ep", "tp")),
        check_vma=False,
    )
```

profile of v0, /device:TPU:0, one launch (start us, length us, event | category | flops | bytes accessed | tf_op | source)
XLA Modules:
  0.0 221.6 jit_solution(14922758619860375159)
XLA Ops:
  7.2 0.0 copy-start
  7.2 0.0 all-gather.6.cloned.1.call-start
  7.2 0.8 broadcast_multiply_fusion
  8.1 0.8 copy.20
  8.9 0.1 eq.29
  9.0 0.1 eq.25
  9.1 1.2 fusion.16
  10.3 0.1 copy.19
  10.4 0.1 mul.502
  10.6 1.1 reduce-window.6
  11.7 0.2 slice_reduce_fusion
  12.0 0.1 fusion.49
  12.1 1.2 fusion.18
  13.3 0.0 copy-start.1
  13.3 12.8 %scatter_custom_fusion = bf16[1024,2048]{1,0:T(8,128)(2,1)} fusion(s32[512]{0:T(512)S(1)} %bitcast.105, bf16[128,2048]{1,0:T(8,128)(2,1)S(1)} %fusion.18, s32[1024]{0:T(1024)S(1)} %pad_clamp_fusion.1, bf16[]{:T(256)} %constant.46.clone.1), kind=kCustom, calls=%fused_computation.39 | custom fusion | bytes 4194306 | tf_op jit(solution)/shard_map/scatter | solution.py:77
  26.1 1.3 constant_dynamic-slice_fusion
  27.4 32.9 %all_to_all.10 = bf16[8,32,2048]{2,1,0:T(8,128)(2,1)} all-to-all(bf16[8,32,2048]{2,1,0:T(8,128)(2,1)S(1)} %constant_dynamic-slice_fusion), channel_id=1, replica_groups=mesh['ep'=8,'tp'=4] {'ep'}, dimensions={0} | all-to-all | bytes 2097152 | tf_op jit(solution)/shard_map/all_to_all | solution.py:82
  60.4 0.0 copy-done.1
  60.4 0.0 all-gather.6.cloned.1.call-update
  60.4 0.0 all-gather.8.cloned.1.call-start
  60.4 33.6 %all-gather.6.cloned.1.call-done = bf16[8,128,2048]{2,1,0:T(8,128)(2,1)} async-done(((bf16[8,32,2048]{2,1,0:T(8,128)(2,1)}), bf16[8,128,2048]{2,1,0:T(8,128)(2,1)}) %all-gather.6.cloned.1.call-update) | async-done | bytes 4194320 | tf_op jit(solution)/shard_map/all_gather | solution.py:83
  94.0 0.0 copy-start.8
  94.0 0.0 copy-start.9
  94.0 7.6 %fusion.2 = f32[1024,1024]{1,0:T(8,128)S(1)} fusion(bf16[1024,2048]{1,0:T(8,128)(2,1)} %bitcast.109, bf16[1,2048,1024]{2,1,0:T(8,128)(2,1)} %param.27), kind=kOutput, calls=%fused_computation.34 | convolution fusion | flops 4294967296 | bytes 12582912 | tf_op jit(solution)/shard_map/dot_general | solution.py:86
  101.7 0.0 copy-done.8
  101.7 0.0 copy-done.9
  101.7 0.0 copy-start.2
  101.7 0.0 copy-start.3
  101.7 0.0 copy-start.4
  101.8 6.3 %multiply_convert_fusion = bf16[1024,1024]{1,0:T(8,128)(2,1)} fusion(f32[1024,1024]{1,0:T(8,128)S(1)} %fusion.2, bf16[1024,2048]{1,0:T(8,128)(2,1)S(1)} %bitcast.110, bf16[1,2048,1024]{2,1,0:T(8,128)(2,1)S(1)} %copy-done.8), kind=kOutput, calls=%fused_computation.38 | convolution fusion | flops 4301258752 | bytes 14680064 | tf_op jit(solution)/shard_map/dot_general | solution.py:85
  108.1 0.0 copy-start.5
  108.1 0.0 copy-start.6
  108.1 0.0 all-gather.8.cloned.1.call-update
  108.1 0.0 all-gather.4.cloned.1.call-start
  108.2 0.0 copy-done.2
  108.2 0.0 copy-done.3
  108.2 0.3 multiply_convert_fusion.2
  108.5 3.4 %collective-permute-start = (bf16[30,512]{1,0:T(8,128)(2,1)S(1)}, bf16[30,512]{1,0:T(8,128)(2,1)S(1)}, u32[]{:S(2)}, u32[]{:S(2)}) collective-permute-start(bf16[30,512]{1,0:T(8,128)(2,1)S(1)} %slice.260), channel_id=1, source_target_pairs={{0,4},{4,8},{8,12},{12,16},{16,20},{20,24},{24,28},{1,5},{5,9},{9,... | collective-permute-start | bytes 92168 | tf_op jit(solution)/shard_map/ppermute | solution.py:10
  111.9 0.0 copy-done.4
  112.0 1.5 collective-permute-done
  113.5 4.8 %fusion.51 = (f32[512]{0:T(512)S(1)}, f32[512]{0:T(512)S(1)}, f32[512,512]{1,0:T(8,128)S(1)}) fusion(bf16[512,512]{1,0:T(8,128)(2,1)S(1)} %multiply_convert_fusion.2, f32[512]{0:T(512)S(1)} %bitcast.103, bf16[30,512]{1,0:T(8,128)(2,1)S(1)} %collective-permute-done, f32[512]{0:T(512)S(1)} %bitcast.104, f32[512]{0:T(512)S(1)} %bitcast.75, ...), kind=kLoop, calls=%fused_computation.113 | loop fusion | flops 48495616 | bytes 1671168 | tf_op jit(solution)/shard_map/reduce_sum | solution.py:44
  118.3 6.5 %all-reduce = (f32[512]{0:T(512)S(1)}, f32[512]{0:T(512)S(1)}) all-reduce(f32[512]{0:T(512)S(1)} %get-tuple-element.3, f32[512]{0:T(512)S(1)} %get-tuple-element.2), channel_id=1, replica_groups=mesh['ep'=8,'tp'=4] {'tp'}, use_global_device_ids=true, to_apply=%region_3.0 | all-reduce | flops 1024 | bytes 8192 | tf_op jit(solution)/shard_map/psum | solution.py:43
  124.8 0.0 copy-done.5
  124.8 0.0 copy-done.6
  124.8 1.2 multiply_convert_fusion.1
  126.0 0.0 all-gather.4.cloned.1.call-update
  126.1 0.0 copy-start.7
  126.1 40.6 %all-gather.8.cloned.1.call-done = bf16[1024,4096]{1,0:T(8,128)(2,1)} async-done(((bf16[1024,1024]{1,0:T(8,128)(2,1)}), bf16[1024,4096]{1,0:T(8,128)(2,1)}) %all-gather.8.cloned.1.call-update) | async-done | bytes 8388624 | tf_op jit(solution)/shard_map/all_gather | solution.py:95
  166.7 10.0 %fusion.11 = bf16[1024,512]{1,0:T(8,128)(2,1)} fusion(bf16[1024,4096]{1,0:T(8,128)(2,1)} %all-gather.8.cloned.1.call-done, bf16[1,4096,512]{2,1,0:T(8,128)(2,1)} %param.28), kind=kOutput, calls=%fused_computation.42 | convolution fusion | flops 4295491584 | bytes 13631488 | tf_op jit(solution)/shard_map/dot_general | solution.py:94
  176.7 5.5 %all-to-all-start.1 = ((bf16[8,128,512]{2,1,0:T(8,128)(2,1)}), bf16[8,128,512]{2,1,0:T(8,128)(2,1)S(1)}, u32[]{:S(2)}, u32[]{:S(2)}) async-start(bf16[8,128,512]{2,1,0:T(8,128)(2,1)} %bitcast.73), calls=%async_computation.1 | async-start | bytes 2097152 | tf_op jit(solution)/shard_map/all_to_all | solution.py:105
  182.2 0.0 copy-done.7
  182.2 0.1 copy.22
  182.3 1.5 fusion.54
  183.8 1.5 fusion.15
  185.3 6.1 %all_gather.15 = bf16[128,512]{1,0:T(8,128)(2,1)S(1)} all-gather(bf16[128,128]{1,0:T(8,128)(2,1)S(1)} %fusion.15), channel_id=1, replica_groups=mesh['ep'=8,'tp'=4] {'tp'}, dimensions={1}, use_global_device_ids=true | all-gather | bytes 163840 | tf_op jit(solution)/shard_map/all_gather | solution.py:100
  191.4 0.7 all-gather.4.cloned.1.call-done
  192.1 0.0 copy-done
  192.1 3.6 %convolution_convert_fusion = bf16[512,512]{1,0:T(8,128)(2,1)} fusion(bf16[512,2048]{1,0:T(8,128)(2,1)} %all-gather.4.cloned.1.call-done, bf16[2048,512]{1,0:T(8,128)(2,1)S(1)} %copy-done), kind=kOutput, calls=%fused_computation.45 | convolution fusion | flops 1074003968 | bytes 4718592 | tf_op jit(solution)/shard_map/dot_general | solution.py:53
  195.7 12.7 %all-to-all-done.1 = bf16[8,128,512]{2,1,0:T(8,128)(2,1)S(1)} async-done(((bf16[8,128,512]{2,1,0:T(8,128)(2,1)}), bf16[8,128,512]{2,1,0:T(8,128)(2,1)S(1)}, u32[]{:S(2)}, u32[]{:S(2)}) %all-to-all-start.1) | async-done | bytes 1048608 | tf_op jit(solution)/shard_map/all_to_all | solution.py:105
  208.4 2.6 %gather_fusion = bf16[512,512]{1,0:T(8,128)(2,1)} fusion(bf16[1024,512]{1,0:T(8,128)(2,1)S(1)} %bitcast.71, s32[1024]{0:T(1024)S(1)} %pad_clamp_fusion), kind=kCustom, calls=%fused_computation.1 | custom fusion | bytes 1050624 | tf_op jit(solution)/shard_map/gather | solution.py:108
  211.0 1.4 reshape.133
  212.4 0.7 multiply_reduce_fusion
  213.1 1.9 fusion.14
  (12 shorter events, 0.2 us)
Async XLA Ops:
  7.2 184.9 %copy-start = (bf16[2048,512]{1,0:T(8,128)(2,1)S(1)}, bf16[2048,512]{1,0:T(8,128)(2,1)}, u32[]{:S(2)}) copy-start(bf16[2048,512]{1,0:T(8,128)(2,1)} %param.21) | copy-start | bytes 6291460
  7.2 86.9 %all-gather.6.cloned.1.call-start = ((), (), s32[]{:S(2)}) async-start(), calls=%async_computation.3 | async-start | bytes 5242880 | tf_op jit(solution)/shard_map/all_gather | solution.py:83
  13.3 47.1 %copy-start.1 = (bf16[128,2048]{1,0:T(8,128)(2,1)}, bf16[128,2048]{1,0:T(8,128)(2,1)S(1)}, u32[]{:S(2)}) copy-start(bf16[128,2048]{1,0:T(8,128)(2,1)S(1)} %fusion.18) | copy-start | bytes 1572868
  60.4 106.3 %all-gather.8.cloned.1.call-start = ((), (), s32[]{:S(2)}) async-start(), calls=%async_computation.4 | async-start | bytes 10485760 | tf_op jit(solution)/shard_map/all_gather | solution.py:95
  94.0 7.7 %copy-start.8 = (bf16[1,2048,1024]{2,1,0:T(8,128)(2,1)S(1)}, bf16[1,2048,1024]{2,1,0:T(8,128)(2,1)}, u32[]{:S(2)}) copy-start(bf16[1,2048,1024]{2,1,0:T(8,128)(2,1)} %param.26) | copy-start | bytes 12582916
  94.0 7.7 %copy-start.9 = (bf16[8,128,2048]{2,1,0:T(8,128)(2,1)S(1)}, bf16[8,128,2048]{2,1,0:T(8,128)(2,1)}, u32[]{:S(2)}) copy-start(bf16[8,128,2048]{2,1,0:T(8,128)(2,1)} %all-gather.6.cloned.1.call-done) | copy-start | bytes 12582916
  101.7 6.4 %copy-start.2 = (bf16[512,512]{1,0:T(8,128)(2,1)S(1)}, bf16[512,512]{1,0:T(8,128)(2,1)}, u32[]{:S(2)}) copy-start(bf16[512,512]{1,0:T(8,128)(2,1)} %param.17) | copy-start | bytes 1572868
  101.7 6.4 %copy-start.3 = (bf16[512,512]{1,0:T(8,128)(2,1)S(1)}, bf16[512,512]{1,0:T(8,128)(2,1)}, u32[]{:S(2)}) copy-start(bf16[512,512]{1,0:T(8,128)(2,1)} %param.16) | copy-start | bytes 1572868
  101.7 10.1 %copy-start.4 = (f32[31,512]{1,0:T(8,128)S(1)}, f32[31,512]{1,0:T(8,128)}, u32[]{:S(2)}) copy-start(f32[31,512]{1,0:T(8,128)} %param.18) | copy-start | bytes 190468
  108.1 16.7 %copy-start.5 = (f32[512]{0:T(512)S(1)}, f32[512]{0:T(512)}, u32[]{:S(2)}) copy-start(f32[512]{0:T(512)} %param.20) | copy-start | bytes 6148
  108.1 16.7 %copy-start.6 = (f32[512]{0:T(512)S(1)}, f32[512]{0:T(512)}, u32[]{:S(2)}) copy-start(f32[512]{0:T(512)} %param.19) | copy-start | bytes 6148
  108.1 84.0 %all-gather.4.cloned.1.call-start = ((), (), s32[]{:S(2)}) async-start(), calls=%async_computation.2 | async-start | bytes 2621440 | tf_op jit(solution)/shard_map/all_gather | solution.py:54
  108.5 5.0 %collective-permute-start = (bf16[30,512]{1,0:T(8,128)(2,1)S(1)}, bf16[30,512]{1,0:T(8,128)(2,1)S(1)}, u32[]{:S(2)}, u32[]{:S(2)}) collective-permute-start(bf16[30,512]{1,0:T(8,128)(2,1)S(1)} %slice.260), channel_id=1, source_target_pairs={{0,4},{4,8},{8,12},{12,16},{16,20},{20,24},{24,28},{1,5},{5,9},{9,... | collective-permute-start | bytes 92168 | tf_op jit(solution)/shard_map/ppermute | solution.py:10
  126.1 56.1 %copy-start.7 = (f32[128,4]{0,1:T(4,128)S(1)}, f32[128,4]{0,1:T(4,128)}, u32[]{:S(2)}) copy-start(f32[128,4]{0,1:T(4,128)} %param.25) | copy-start | bytes 6148
  176.7 31.7 %all-to-all-start.1 = ((bf16[8,128,512]{2,1,0:T(8,128)(2,1)}), bf16[8,128,512]{2,1,0:T(8,128)(2,1)S(1)}, u32[]{:S(2)}, u32[]{:S(2)}) async-start(bf16[8,128,512]{2,1,0:T(8,128)(2,1)} %bitcast.73), calls=%async_computation.1 | async-start | bytes 2097152 | tf_op jit(solution)/shard_map/all_to_all | solution.py:105
Sparse Core Ops, SparseCore 0:
  60.5 33.4 all-gather.5
  108.2 58.3 all-gather.7
  168.8 23.2 all-gather.3
where the time goes:
time: 222 us
  waiting for transfers between devices  89.1 us (40%)
  blocking collectives  45.5 us (20%)
  matrix products  32.5 us (15%)
  local copies, waits for them, and re-layouts  19.8 us (9%)
  between operations  14 us (6%)
  other arithmetic  11.7 us (5%)
  starting transfers between devices  9.02 us (4%)
    all_gather x1, waiting for transfers between devices, body(): lax.all_gather(expert_hidden, 'tp', axis=1, tiled=True)  40.6 us
    all_gather x1, waiting for transfers between devices, body(): arrived = lax.all_gather(partial_rows, 'tp', axis=1, tiled=True)  33.6 us
    all_to_all x1, blocking collectives, body(): lax.all_to_all(own_slots, 'ep', split_axis=0, concat_axis=0, tiled=True)  32.9 us
    scatter x1, local copies, waits for them, and re-layouts, body(): outgoing = jnp.zeros((groups * capacity, model_width), jnp.bfloat16).at[s...  12.8 us
    all_to_all x1, waiting for transfers between devices, body(): lax.all_to_all(expert_out, 'ep', split_axis=0, concat_axis=0, tiled=True)  12.7 us
    dot_general x1, matrix products, body(): jnp.dot(lax.all_gather(expert_hidden, 'tp', axis=1, tiled=True), routed_r...  10 us
    dot_general x1, matrix products, body(): jnp.dot(arrived_rows, expert_up[0], preferred_element_type=jnp.float32)  7.64 us
    psum x1, blocking collectives, body(): lax.psum((jnp.sum(filtered, axis=1), jnp.sum(filtered * filtered, axis=1)...  6.48 us
  transfers between devices with their start and end apart: 5, of which 5 were waited for; matrix products, arithmetic and copies ran while one was open for 10% of the time, Pallas kernels for 0%

commit v1 on v0

--- a/solution.py
+++ b/solution.py
@@ -92,7 +92,7 @@
     columns = expert_down.shape[2]
     routed_rows = expert_down[0]
     routed_sum = jnp.dot(
-        lax.all_gather(expert_hidden, "tp", axis=1, tiled=True),
+        jnp.concatenate(lax.all_gather(expert_hidden, "tp"), axis=1),
         routed_rows,
         preferred_element_type=jnp.float32,
     )

time: 222 us -> 234 us (1.054)
  local copies, waits for them, and re-layouts: 19.8 us -> 31.2 us
    all_gather x0 -> x1, local copies, waits for them, and re-layouts: none -> 11.5 us  [body(): lax.all_gather(expert_hidden, 'tp')]
  transfers between devices with their start and end apart: 5 -> 5, of which waited for: 5 -> 4; matrix products, arithmetic and copies ran while one was open for 10% -> 15% of each run, Pallas kernels for 0% -> 0%
where the time goes in v1:
time: 234 us; the launch traced here: 233 us
  waiting for transfers between devices  89.6 us (38%)
  blocking collectives  45.1 us (19%)
  matrix products  32.7 us (14%)
  local copies, waits for them, and re-layouts  31.2 us (13%)
  between operations  14 us (6%)
  other arithmetic  11.7 us (5%)
  starting transfers between devices  9.01 us (4%)
    all_gather x1, waiting for transfers between devices, body(): lax.all_gather(expert_hidden, 'tp')  40.6 us
    all_gather x1, waiting for transfers between devices, body(): arrived = lax.all_gather(partial_rows, 'tp', axis=1, tiled=True)  33.6 us
    all_to_all x1, blocking collectives, body(): lax.all_to_all(own_slots, 'ep', split_axis=0, concat_axis=0, tiled=True)  32.9 us
    all_to_all x1, waiting for transfers between devices, body(): lax.all_to_all(expert_out, 'ep', split_axis=0, concat_axis=0, tiled=True)  13.8 us
    scatter x1, local copies, waits for them, and re-layouts, body(): outgoing = jnp.zeros((groups * capacity, model_width), jnp.bfloat16).at[s...  12.8 us
    all_gather x1, local copies, waits for them, and re-layouts, body(): lax.all_gather(expert_hidden, 'tp')  11.5 us
    dot_general x1, matrix products, body(): jnp.dot(jnp.concatenate(lax.all_gather(expert_hidden, 'tp'), axis=1), rou...  10.1 us
    dot_general x1, matrix products, body(): jnp.dot(arrived_rows, expert_up[0], preferred_element_type=jnp.float32)  7.64 us
  transfers between devices with their start and end apart: 5, of which 4 were waited for; matrix products, arithmetic and copies ran while one was open for 15% of the time, Pallas kernels for 0%

profile of v1, /device:TPU:0, one launch (start us, length us, event | category | flops | bytes accessed | tf_op | source)
XLA Modules:
  0.0 233.2 jit_solution(5762401831842666973)
XLA Ops:
  7.2 0.0 copy-start
  7.2 0.0 all-gather.7.cloned.1.call-start
  7.2 0.8 broadcast_multiply_fusion
  8.1 0.8 copy.20
  8.9 0.1 eq.29
  9.0 0.1 eq.25
  9.1 1.2 fusion.16
  10.3 0.1 copy.19
  10.4 0.1 mul.502
  10.6 1.1 reduce-window.6
  11.7 0.2 slice_reduce_fusion
  12.0 0.1 fusion.49
  12.1 1.2 fusion.18
  13.3 0.0 copy-start.1
  13.3 12.8 %scatter_custom_fusion = bf16[1024,2048]{1,0:T(8,128)(2,1)} fusion(s32[512]{0:T(512)S(1)} %bitcast.111, bf16[128,2048]{1,0:T(8,128)(2,1)S(1)} %fusion.18, s32[1024]{0:T(1024)S(1)} %pad_clamp_fusion.1, bf16[]{:T(256)} %constant.46.clone.1), kind=kCustom, calls=%fused_computation.39 | custom fusion | bytes 4194306 | tf_op jit(solution)/shard_map/scatter | solution.py:77
  26.1 1.3 constant_dynamic-slice_fusion
  27.4 32.9 %all_to_all.10 = bf16[8,32,2048]{2,1,0:T(8,128)(2,1)} all-to-all(bf16[8,32,2048]{2,1,0:T(8,128)(2,1)S(1)} %constant_dynamic-slice_fusion), channel_id=1, replica_groups=mesh['ep'=8,'tp'=4] {'ep'}, dimensions={0} | all-to-all | bytes 2097152 | tf_op jit(solution)/shard_map/all_to_all | solution.py:82
  60.4 0.0 copy-done.1
  60.4 0.0 all-gather.7.cloned.1.call-update
  60.4 0.0 all-gather.9.cloned.1.call-start
  60.4 33.6 %all-gather.7.cloned.1.call-done = bf16[8,128,2048]{2,1,0:T(8,128)(2,1)} async-done(((bf16[8,32,2048]{2,1,0:T(8,128)(2,1)}), bf16[8,128,2048]{2,1,0:T(8,128)(2,1)}) %all-gather.7.cloned.1.call-update) | async-done | bytes 4194320 | tf_op jit(solution)/shard_map/all_gather | solution.py:83
  94.0 0.0 copy-start.8
  94.0 0.0 copy-start.9
  94.0 7.6 %fusion.2 = f32[1024,1024]{1,0:T(8,128)S(1)} fusion(bf16[1024,2048]{1,0:T(8,128)(2,1)} %bitcast.115, bf16[1,2048,1024]{2,1,0:T(8,128)(2,1)} %param.27), kind=kOutput, calls=%fused_computation.34 | convolution fusion | flops 4294967296 | bytes 12582912 | tf_op jit(solution)/shard_map/dot_general | solution.py:86
  101.7 0.0 copy-done.8
  101.7 0.0 copy-done.9
  101.7 0.0 copy-start.2
  101.7 0.0 copy-start.3
  101.7 0.0 copy-start.4
  101.8 6.4 %multiply_convert_fusion = bf16[1024,1024]{1,0:T(8,128)(2,1)} fusion(f32[1024,1024]{1,0:T(8,128)S(1)} %fusion.2, bf16[1024,2048]{1,0:T(8,128)(2,1)S(1)} %bitcast.116, bf16[1,2048,1024]{2,1,0:T(8,128)(2,1)S(1)} %copy-done.8), kind=kOutput, calls=%fused_computation.38 | convolution fusion | flops 4301258752 | bytes 14680064 | tf_op jit(solution)/shard_map/dot_general | solution.py:85
  108.1 0.0 copy-start.5
  108.1 0.0 copy-start.6
  108.1 0.0 all-gather.9.cloned.1.call-update
  108.2 0.0 all-gather.5.cloned.1.call-start
  108.2 0.0 copy-done.2
  108.2 0.0 copy-done.3
  108.2 0.3 multiply_convert_fusion.2
  108.5 3.4 %collective-permute-start = (bf16[30,512]{1,0:T(8,128)(2,1)S(1)}, bf16[30,512]{1,0:T(8,128)(2,1)S(1)}, u32[]{:S(2)}, u32[]{:S(2)}) collective-permute-start(bf16[30,512]{1,0:T(8,128)(2,1)S(1)} %slice.260), channel_id=1, source_target_pairs={{0,4},{4,8},{8,12},{12,16},{16,20},{20,24},{24,28},{1,5},{5,9},{9,... | collective-permute-start | bytes 92168 | tf_op jit(solution)/shard_map/ppermute | solution.py:10
  111.9 0.0 copy-done.4
  112.0 1.5 collective-permute-done
  113.5 4.8 %fusion.51 = (f32[512]{0:T(512)S(1)}, f32[512]{0:T(512)S(1)}, f32[512,512]{1,0:T(8,128)S(1)}) fusion(bf16[512,512]{1,0:T(8,128)(2,1)S(1)} %multiply_convert_fusion.2, f32[512]{0:T(512)S(1)} %bitcast.109, bf16[30,512]{1,0:T(8,128)(2,1)S(1)} %collective-permute-done, f32[512]{0:T(512)S(1)} %bitcast.110, f32[512]{0:T(512)S(1)} %bitcast.81, ...), kind=kLoop, calls=%fused_computation.113 | loop fusion | flops 48495616 | bytes 1671168 | tf_op jit(solution)/shard_map/reduce_sum | solution.py:44
  118.4 6.5 %all-reduce = (f32[512]{0:T(512)S(1)}, f32[512]{0:T(512)S(1)}) all-reduce(f32[512]{0:T(512)S(1)} %get-tuple-element.3, f32[512]{0:T(512)S(1)} %get-tuple-element.2), channel_id=1, replica_groups=mesh['ep'=8,'tp'=4] {'tp'}, use_global_device_ids=true, to_apply=%region_3.0 | all-reduce | flops 1024 | bytes 8192 | tf_op jit(solution)/shard_map/psum | solution.py:43
  124.9 0.0 copy-done.5
  124.9 0.0 copy-done.6
  124.9 1.2 multiply_convert_fusion.1
  126.1 0.0 all-gather.5.cloned.1.call-update
  126.1 40.6 %all-gather.9.cloned.1.call-done = bf16[4096,1024]{1,0:T(8,128)(2,1)} async-done(((bf16[1024,1024]{1,0:T(8,128)(2,1)}), bf16[4096,1024]{1,0:T(8,128)(2,1)}) %all-gather.9.cloned.1.call-update) | async-done | bytes 8388624 | tf_op jit(solution)/shard_map/all_gather | solution.py:95
  166.7 11.5 %copy.22 = bf16[4,1024,1024]{1,2,0:T(8,128)(2,1)} copy(bf16[4,1024,1024]{2,1,0:T(8,128)(2,1)} %bitcast.76) | data formatting | bytes 16777216 | tf_op jit(solution)/shard_map/all_gather | solution.py:95
  178.2 0.0 copy-start.7
  178.2 10.1 %fusion.11 = bf16[1024,512]{1,0:T(8,128)(2,1)} fusion(bf16[1024,4096]{0,1:T(8,128)(2,1)} %bitcast.77, bf16[1,4096,512]{2,1,0:T(8,128)(2,1)} %param.28), kind=kOutput, calls=%fused_computation.42 | convolution fusion | flops 4295491584 | bytes 13631488 | tf_op jit(solution)/shard_map/dot_general | solution.py:94
  188.3 5.5 %all-to-all-start.1 = ((bf16[8,128,512]{2,1,0:T(8,128)(2,1)}), bf16[8,128,512]{2,1,0:T(8,128)(2,1)S(1)}, u32[]{:S(2)}, u32[]{:S(2)}) async-start(bf16[8,128,512]{2,1,0:T(8,128)(2,1)} %bitcast.79), calls=%async_computation.1 | async-start | bytes 2097152 | tf_op jit(solution)/shard_map/all_to_all | solution.py:105
  193.8 0.0 copy-done.7
  193.8 0.1 copy.23
  193.9 1.5 fusion.54
  195.4 1.5 fusion.15
  196.9 5.7 %all_gather.19 = bf16[128,512]{1,0:T(8,128)(2,1)S(1)} all-gather(bf16[128,128]{1,0:T(8,128)(2,1)S(1)} %fusion.15), channel_id=1, replica_groups=mesh['ep'=8,'tp'=4] {'tp'}, dimensions={1}, use_global_device_ids=true | all-gather | bytes 163840 | tf_op jit(solution)/shard_map/all_gather | solution.py:100
  202.6 0.0 all-gather.5.cloned.1.call-done
  202.6 0.0 copy-done
  202.6 3.6 %convolution_convert_fusion = bf16[512,512]{1,0:T(8,128)(2,1)} fusion(bf16[512,2048]{1,0:T(8,128)(2,1)} %all-gather.5.cloned.1.call-done, bf16[2048,512]{1,0:T(8,128)(2,1)S(1)} %copy-done), kind=kOutput, calls=%fused_computation.45 | convolution fusion | flops 1074003968 | bytes 4718592 | tf_op jit(solution)/shard_map/dot_general | solution.py:53
  206.2 13.8 %all-to-all-done.1 = bf16[8,128,512]{2,1,0:T(8,128)(2,1)S(1)} async-done(((bf16[8,128,512]{2,1,0:T(8,128)(2,1)}), bf16[8,128,512]{2,1,0:T(8,128)(2,1)S(1)}, u32[]{:S(2)}, u32[]{:S(2)}) %all-to-all-start.1) | async-done | bytes 1048608 | tf_op jit(solution)/shard_map/all_to_all | solution.py:105
  220.0 2.6 %gather_fusion = bf16[512,512]{1,0:T(8,128)(2,1)} fusion(bf16[1024,512]{1,0:T(8,128)(2,1)S(1)} %bitcast.75, s32[1024]{0:T(1024)S(1)} %pad_clamp_fusion), kind=kCustom, calls=%fused_computation.1 | custom fusion | bytes 1050624 | tf_op jit(solution)/shard_map/gather | solution.py:108
  222.6 1.4 reshape.141
  224.0 0.7 multiply_reduce_fusion
  224.7 1.9 fusion.14
  (12 shorter events, 0.2 us)
Async XLA Ops:
  7.2 195.4 %copy-start = (bf16[2048,512]{1,0:T(8,128)(2,1)S(1)}, bf16[2048,512]{1,0:T(8,128)(2,1)}, u32[]{:S(2)}) copy-start(bf16[2048,512]{1,0:T(8,128)(2,1)} %param.21) | copy-start | bytes 6291460
  7.2 86.9 %all-gather.7.cloned.1.call-start = ((), (), s32[]{:S(2)}) async-start(), calls=%async_computation.3 | async-start | bytes 5242880 | tf_op jit(solution)/shard_map/all_gather | solution.py:83
  13.3 47.1 %copy-start.1 = (bf16[128,2048]{1,0:T(8,128)(2,1)}, bf16[128,2048]{1,0:T(8,128)(2,1)S(1)}, u32[]{:S(2)}) copy-start(bf16[128,2048]{1,0:T(8,128)(2,1)S(1)} %fusion.18) | copy-start | bytes 1572868
  60.4 106.3 %all-gather.9.cloned.1.call-start = ((), (), s32[]{:S(2)}) async-start(), calls=%async_computation.4 | async-start | bytes 10485760 | tf_op jit(solution)/shard_map/all_gather | solution.py:95
  94.0 7.7 %copy-start.8 = (bf16[1,2048,1024]{2,1,0:T(8,128)(2,1)S(1)}, bf16[1,2048,1024]{2,1,0:T(8,128)(2,1)}, u32[]{:S(2)}) copy-start(bf16[1,2048,1024]{2,1,0:T(8,128)(2,1)} %param.26) | copy-start | bytes 12582916
  94.0 7.7 %copy-start.9 = (bf16[8,128,2048]{2,1,0:T(8,128)(2,1)S(1)}, bf16[8,128,2048]{2,1,0:T(8,128)(2,1)}, u32[]{:S(2)}) copy-start(bf16[8,128,2048]{2,1,0:T(8,128)(2,1)} %all-gather.7.cloned.1.call-done) | copy-start | bytes 12582916
  101.7 6.5 %copy-start.2 = (bf16[512,512]{1,0:T(8,128)(2,1)S(1)}, bf16[512,512]{1,0:T(8,128)(2,1)}, u32[]{:S(2)}) copy-start(bf16[512,512]{1,0:T(8,128)(2,1)} %param.17) | copy-start | bytes 1572868
  101.7 6.5 %copy-start.3 = (bf16[512,512]{1,0:T(8,128)(2,1)S(1)}, bf16[512,512]{1,0:T(8,128)(2,1)}, u32[]{:S(2)}) copy-start(bf16[512,512]{1,0:T(8,128)(2,1)} %param.16) | copy-start | bytes 1572868
  101.7 10.2 %copy-start.4 = (f32[31,512]{1,0:T(8,128)S(1)}, f32[31,512]{1,0:T(8,128)}, u32[]{:S(2)}) copy-start(f32[31,512]{1,0:T(8,128)} %param.18) | copy-start | bytes 190468
  108.1 16.7 %copy-start.5 = (f32[512]{0:T(512)S(1)}, f32[512]{0:T(512)}, u32[]{:S(2)}) copy-start(f32[512]{0:T(512)} %param.20) | copy-start | bytes 6148
  108.1 16.7 %copy-start.6 = (f32[512]{0:T(512)S(1)}, f32[512]{0:T(512)}, u32[]{:S(2)}) copy-start(f32[512]{0:T(512)} %param.19) | copy-start | bytes 6148
  108.2 94.4 %all-gather.5.cloned.1.call-start = ((), (), s32[]{:S(2)}) async-start(), calls=%async_computation.2 | async-start | bytes 2621440 | tf_op jit(solution)/shard_map/all_gather | solution.py:54
  108.5 5.0 %collective-permute-start = (bf16[30,512]{1,0:T(8,128)(2,1)S(1)}, bf16[30,512]{1,0:T(8,128)(2,1)S(1)}, u32[]{:S(2)}, u32[]{:S(2)}) collective-permute-start(bf16[30,512]{1,0:T(8,128)(2,1)S(1)} %slice.260), channel_id=1, source_target_pairs={{0,4},{4,8},{8,12},{12,16},{16,20},{20,24},{24,28},{1,5},{5,9},{9,... | collective-permute-start | bytes 92168 | tf_op jit(solution)/shard_map/ppermute | solution.py:10
  178.2 15.6 %copy-start.7 = (f32[128,4]{0,1:T(4,128)S(1)}, f32[128,4]{0,1:T(4,128)}, u32[]{:S(2)}) copy-start(f32[128,4]{0,1:T(4,128)} %param.25) | copy-start | bytes 6148
  188.3 31.7 %all-to-all-start.1 = ((bf16[8,128,512]{2,1,0:T(8,128)(2,1)}), bf16[8,128,512]{2,1,0:T(8,128)(2,1)S(1)}, u32[]{:S(2)}, u32[]{:S(2)}) async-start(bf16[8,128,512]{2,1,0:T(8,128)(2,1)} %bitcast.79), calls=%async_computation.1 | async-start | bytes 2097152 | tf_op jit(solution)/shard_map/all_to_all | solution.py:105
Sparse Core Ops, SparseCore 0:
  60.5 33.4 all-gather.6
  108.3 58.3 all-gather.8
  168.9 22.5 all-gather.4
